TPU v7x, 32 devices: a whole 2x2x4 slice. The times are simulated.
32 devices in a mesh: fs: 8 (over z, y), tp: 4 (over x, core).
Axes of the slice: x: 2, y: 2, z: 4, core: 2. Of those that a mesh axis runs over, the one named last changes fastest.
Arguments:
- tokens: bfloat16 [6144, 2048], P('fs'), may hold values from -6 to 6
- routes: int32 [6144, 2], P('fs'), may hold values from 0 to 7, all different within a row; in each aligned block of 768 rows (0 to 767, 768 to 1535, ...) at most 216 rows name the same one
- route_weight: float32 [6144, 2], P('fs'), may hold values from 0.2 to 1
- norm_gain: float32 [2048], P('fs'), may hold values from 0.1 to 1.9
- gate_master: float32 [8, 2048, 4096], P(None, 'fs', 'tp'), may hold values from -0.125 to 0.125
- up_master: float32 [8, 2048, 4096], P(None, 'fs', 'tp'), may hold values from -0.125 to 0.125
- down_master: float32 [8, 4096, 2048], P(None, 'fs', 'tp'), may hold values from -0.09375 to 0.09375
Outputs:
- gate_serve: bfloat16 [8, 2048, 4096], P('fs', None, 'tp')
- up_serve: bfloat16 [8, 2048, 4096], P('fs', None, 'tp')
- down_serve: bfloat16 [8, 4096, 2048], P('fs', 'tp')
- layer_out: bfloat16 [6144, 2048], P('fs', 'tp')
Inputs may be any that keep to these rules, and one draw needn't show every extreme that they name: `routes`: each row names two different experts; among the 768 rows of one index of fs no expert is named by more than 216 rows, a bound that some block reaches.
All inputs are finite; a program needn't handle non-finite values.
Results may differ from a plain program's by a relative error of at most 0.015.
Values may be sent and summed in bfloat16 or wider, within the bound.
A program may use at most 192 MiB of HBM per device.

v0:
```python
import jax
import jax.numpy as jnp
from jax import lax
from jax.sharding import PartitionSpec as P

CAP = 216


def relay_down(down_cast):
    return lax.all_to_all(
        lax.all_to_all(down_cast, "fs", split_axis=0, concat_axis=1, tiled=True),
        "tp",
        split_axis=1,
        concat_axis=2,
        tiled=True,
    )


def body(tokens, routes, route_weight, norm_gain, gate_master, up_master, down_master):
    rows_local = tokens.shape[0]
    model_width = tokens.shape[1]
    experts = gate_master.shape[0]
    values = tokens.astype(jnp.float32)
    normed = (values * lax.rsqrt(jnp.mean(values * values, axis=-1, keepdims=True) + 1e-06)).astype(
        jnp.bfloat16
    )
    row_gain = norm_gain[None, :, None]
    gate_cast = (row_gain * gate_master).astype(jnp.bfloat16)
    up_cast = (row_gain * up_master).astype(jnp.bfloat16)
    down_cast = down_master.astype(jnp.bfloat16)
    gate_serve, up_serve = (
        lax.all_to_all(gate_cast, "fs", split_axis=0, concat_axis=1, tiled=True),
        lax.all_to_all(up_cast, "fs", split_axis=0, concat_axis=1, tiled=True),
    )
    down_serve = relay_down(down_cast)
    chosen = routes.reshape(-1)
    one_hot = (chosen[:, None] == jnp.arange(experts, dtype=jnp.int32)[None, :]).astype(jnp.int32)
    earlier = jnp.cumsum(one_hot, axis=0) - one_hot
    position = jnp.sum(earlier * one_hot, axis=1)
    slot_index = chosen * CAP + position
    doubled = jnp.repeat(normed, 2, axis=0)
    outgoing = jnp.zeros((experts * CAP, model_width), jnp.bfloat16).at[slot_index].set(doubled)
    outgoing = outgoing.reshape(experts, CAP, model_width)
    gate_matrix = gate_serve[0]
    up_matrix = up_serve[0]
    column_count = model_width // lax.axis_size("tp")
    column_share = lax.dynamic_slice_in_dim(
        outgoing, lax.axis_index("tp") * column_count, column_count, 2
    )
    arrived = lax.all_to_all(column_share, "fs", split_axis=0, concat_axis=0, tiled=True)
    stacked = arrived.reshape(-1, column_count)
    incoming = lax.all_gather(stacked, "tp", axis=1, tiled=True)
    gate_pre = jnp.dot(incoming, gate_matrix, preferred_element_type=jnp.float32)
    up_pre = jnp.dot(incoming, up_matrix, preferred_element_type=jnp.float32)
    hidden = (jax.nn.silu(gate_pre) * up_pre).astype(jnp.bfloat16)
    partial_value = jnp.dot(hidden, down_serve[0], preferred_element_type=jnp.float32)
    rounded = lax.optimization_barrier(partial_value.astype(jnp.bfloat16)).astype(jnp.float32)
    rounded = rounded.reshape(-1, CAP, model_width)
    summed = lax.psum_scatter(rounded.astype(jnp.bfloat16), "tp", scatter_dimension=2, tiled=True)
    returned = lax.all_to_all(summed, "fs", split_axis=0, concat_axis=0, tiled=True)
    returned_rows = returned.reshape(experts * CAP, -1)
    picked = returned_rows[slot_index].astype(jnp.float32).reshape(rows_local, 2, -1)
    combined = jnp.sum(picked * route_weight[:, :, None], axis=1).astype(jnp.bfloat16)
    return (gate_serve, up_serve, down_serve, combined)


def solution(mesh):
    placed = (
        P("fs", None),
        P("fs", None),
        P("fs", None),
        P("fs"),
        P(None, "fs", "tp"),
        P(None, "fs", "tp"),
        P(None, "fs", "tp"),
    )
    return jax.shard_map(
        body,
        mesh=mesh,
        in_specs=placed,
        out_specs=(P("fs", None, "tp"), P("fs", None, "tp"), P("fs", "tp", None), P("fs", "tp")),
        check_vma=False,
    )
```

profile of v0, /device:TPU:0, one launch (start us, length us, event | category | flops | bytes accessed | tf_op | source)
XLA Modules:
  0.0 605.9 jit_solution(8476485770891037093)
XLA Ops:
  7.2 0.0 copy-start
  7.2 1.0 copy.33
  8.2 0.2 eq.29
  8.4 0.2 eq.25
  8.7 1.3 broadcast_multiply_fusion
  10.0 2.3 reduce-window.6
  12.2 0.3 slice_reduce_fusion
  12.5 0.2 reduce-window.9
  12.7 0.7 add_bitcast_fusion
  13.4 0.9 copy.32
  14.3 0.3 mul.67
  14.5 2.6 fusion
  17.1 0.0 copy-done
  17.1 0.6 fusion.1
  17.7 5.2 broadcast_in_dim.5
  22.9 0.0 copy-start.2
  22.9 10.2 %reshape.112 = bf16[1536,2048]{1,0:T(8,128)(2,1)} reshape(bf16[768,2,2048]{2,1,0:T(2,128)(2,1)} %broadcast_in_dim.5) | data formatting | bytes 12582912 | tf_op jit(solution)/shard_map/reshape | solution.py:41
  33.2 0.0 copy-done.2
  33.2 14.5 %scatter_custom_fusion = bf16[1728,2048]{1,0:T(8,128)(2,1)} fusion(s32[1536]{0:T(1024)S(1)} %fusion.9, bf16[1536,2048]{1,0:T(8,128)(2,1)} %reshape.112, bf16[]{:T(256)} %constant.11.clone.1), kind=kCustom, calls=%fused_computation.11 | custom fusion | bytes 7078400 | tf_op jit(solution)/shard_map/scatter | solution.py:42
  47.7 2.8 constant_dynamic-slice_fusion
  50.5 7.3 %all-to-all-start.4 = ((bf16[8,216,512]{2,1,0:T(8,128)(2,1)}), bf16[8,216,512]{2,1,0:T(8,128)(2,1)S(1)}, u32[]{:S(2)}, u32[]{:S(2)}) async-start(bf16[8,216,512]{2,1,0:T(8,128)(2,1)} %constant_dynamic-slice_fusion), calls=%async_computation.4 | async-start | bytes 3538944 | tf_op jit(solution)/shard_map/all_to_all | solution.py:50
  57.8 5.9 convert_element_type.45
  63.7 0.0 copy-start.4
  63.7 35.3 %all-to-all-done.4 = bf16[8,216,512]{2,1,0:T(8,128)(2,1)S(1)} async-done(((bf16[8,216,512]{2,1,0:T(8,128)(2,1)}), bf16[8,216,512]{2,1,0:T(8,128)(2,1)S(1)}, u32[]{:S(2)}, u32[]{:S(2)}) %all-to-all-start.4) | async-done | bytes 1769504 | tf_op jit(solution)/shard_map/all_to_all | solution.py:50
  99.0 0.0 copy-start.1
  99.0 4.8 all-to-all-start.2
  103.8 0.0 copy-done.4
  103.8 11.9 %multiply_convert_fusion = (bf16[8,256,1024]{2,1,0:T(8,128)(2,1)}, bf16[8,256,1024]{2,1,0:T(8,128)(2,1)}) fusion(f32[8,256,1024]{2,1,0:T(8,128)} %param.12, f32[256]{0:T(256)S(1)} %copy-done.4, f32[8,256,1024]{2,1,0:T(8,128)} %param.11), kind=kLoop, calls=%fused_computation.2 | loop fusion | flops 8388608 | bytes 25166848 | tf_op jit(solution)/shard_map/convert_element_type | solution.py:29
  115.7 0.0 copy-done.1
  115.7 80.4 %all-to-all-done.2 = bf16[8,512,512]{2,1,0:T(8,128)(2,1)} async-done(((bf16[8,512,512]{2,1,0:T(8,128)(2,1)}), bf16[8,512,512]{2,1,0:T(8,128)(2,1)}, u32[]{:S(2)}, u32[]{:S(2)}) %all-to-all-start.2) | async-done | bytes 4194336 | tf_op jit(solution)/shard_map/all_to_all | solution.py:11
  196.2 4.6 all-to-all-start
  200.7 0.0 all-gather.2.cloned.1.call-start
  200.8 0.7 all-gather.2.cloned.1.call-update
  201.5 8.6 %copy.42 = bf16[1,4096,512]{2,0,1:T(2,128)(2,1)} copy(bf16[1,4096,512]{2,1,0:T(8,128)(2,1)} %bitcast.2) | data formatting | bytes 8388608 | tf_op jit(solution)/shard_map/all_to_all | solution.py:11
  210.1 0.5 broadcast.72
  210.6 28.6 %reduce.4 = bf16[4096,512]{1,0:T(8,128)(2,1)} reduce(bf16[4096,1,512]{2,1,0:T(2,128)(2,1)} %bitcast.43, bf16[]{:T(256)} %broadcast.72), dimensions={1}, to_apply=%bitcast.40.reduce_sub_computation | reduce | bytes 8388610
  239.2 6.2 %reshape.120 = bf16[4,2,262144]{2,1,0:T(2,128)(2,1)} reshape(bf16[4096,512]{1,0:T(8,128)(2,1)} %reduce.4) | data formatting | bytes 8388608
  245.5 47.7 %all-to-all-done = bf16[8,256,1024]{2,1,0:T(8,128)(2,1)} async-done(((bf16[8,256,1024]{2,1,0:T(8,128)(2,1)}), bf16[8,256,1024]{2,1,0:T(8,128)(2,1)}, u32[]{:S(2)}, u32[]{:S(2)}) %all-to-all-start) | async-done | bytes 4194336 | tf_op jit(solution)/shard_map/all_to_all | solution.py:32
  293.1 53.8 %all_to_all.64 = bf16[4,2,262144]{2,1,0:T(2,128)(2,1)} all-to-all(bf16[4,2,262144]{2,1,0:T(2,128)(2,1)} %reshape.120), channel_id=1, replica_groups=mesh['fs'=8,'tp'=4] {'tp'}, dimensions={0} | all-to-all | bytes 8388608 | tf_op jit(solution)/shard_map/all_to_all | solution.py:10
  347.0 4.5 all-to-all-start.1
  351.5 0.3 reduce-scatter.2.cloned.1.call-start
  351.8 7.4 %reshape.121 = bf16[4096,1,512]{2,1,0:T(2,128)(2,1)} reshape(bf16[4,2,262144]{2,1,0:T(2,128)(2,1)} %all_to_all.64) | data formatting | bytes 8388608
  359.2 6.6 %copy.38 = bf16[1,4096,512]{2,1,0:T(8,128)(2,1)} copy(bf16[1,4096,512]{2,0,1:T(2,128)(2,1)} %bitcast.44) | data formatting | bytes 8388608
  365.9 6.2 %copy.31 = bf16[1,1024,4,512]{1,3,2,0:T(8,128)(2,1)} copy(bf16[1,1024,4,512]{3,1,2,0:T(8,128)(2,1)} %bitcast.45) | data formatting | bytes 8388608 | tf_op jit(solution)/shard_map/all_to_all | solution.py:10
  372.1 0.0 all-gather.2.cloned.1.call-done
  372.1 12.7 %fusion.11 = f32[1728,1024]{1,0:T(8,128)} fusion(bf16[1728,2048]{1,0:T(8,128)(2,1)} %all-gather.2.cloned.1.call-done, bf16[2048,1024]{1,0:T(8,128)(2,1)} %bitcast.8), kind=kOutput, calls=%fused_computation.31 | convolution fusion | flops 7247757312 | bytes 18350080 | tf_op jit(solution)/shard_map/dot_general | solution.py:53
  384.8 59.8 %all-to-all-done.1 = bf16[8,256,1024]{2,1,0:T(8,128)(2,1)} async-done(((bf16[8,256,1024]{2,1,0:T(8,128)(2,1)}), bf16[8,256,1024]{2,1,0:T(8,128)(2,1)}, u32[]{:S(2)}, u32[]{:S(2)}) %all-to-all-start.1) | async-done | bytes 4194336 | tf_op jit(solution)/shard_map/all_to_all | solution.py:33
  444.6 22.6 %convolution_convert_fusion = bf16[1728,2048]{1,0:T(8,128)(2,1)} fusion(bf16[1024,2048]{0,1:T(8,128)(2,1)} %bitcast.46, f32[1728,1024]{1,0:T(8,128)} %fusion.11, bf16[1728,2048]{1,0:T(8,128)(2,1)} %all-gather.2.cloned.1.call-done, bf16[2048,1024]{1,0:T(8,128)(2,1)} %bitcast.9), kind=kOutput, calls=%fused_computation.6 | convolution fusion | flops 14509670400 | bytes 29622272 | tf_op jit(solution)/shard_map/dot_general | solution.py:56
  467.2 0.0 copy-start.3
  467.2 0.0 reduce-scatter.2.cloned.1.call-update
  467.2 61.4 %reduce-scatter.2.cloned.1.call-done = bf16[8,216,512]{2,1,0:T(8,128)(2,1)} async-done(((bf16[8,216,2048]{2,1,0:T(8,128)(2,1)}), bf16[8,216,512]{2,1,0:T(8,128)(2,1)}) %reduce-scatter.2.cloned.1.call-update) | async-done | bytes 1769488 | tf_op jit(solution)/shard_map/reduce_scatter | solution.py:59
  528.7 5.5 all-to-all-start.5
  534.2 0.0 copy-done.3
  534.2 0.2 copy.36
  534.4 6.4 %copy.37 = bf16[1,1024,2048]{2,1,0:T(8,128)(2,1)} copy(bf16[1,1024,2048]{1,2,0:T(8,128)(2,1)} %bitcast.47) | data formatting | bytes 8388608
  540.8 34.4 %all-to-all-done.5 = bf16[8,216,512]{2,1,0:T(8,128)(2,1)S(1)} async-done(((bf16[8,216,512]{2,1,0:T(8,128)(2,1)}), bf16[8,216,512]{2,1,0:T(8,128)(2,1)S(1)}, u32[]{:S(2)}, u32[]{:S(2)}) %all-to-all-start.5) | async-done | bytes 1769504 | tf_op jit(solution)/shard_map/all_to_all | solution.py:60
  575.3 5.4 gather_fusion
  580.7 3.4 reshape.99
  584.1 5.7 multiply_reduce_fusion
  589.8 4.6 copy.45
  594.4 4.6 copy.46
  (5 shorter events, 0.1 us)
Async XLA Ops:
  7.2 10.0 %copy-start = (bf16[768,2048]{1,0:T(8,128)(2,1)S(1)}, bf16[768,2048]{1,0:T(8,128)(2,1)}, u32[]{:S(2)}) copy-start(bf16[768,2048]{1,0:T(8,128)(2,1)} %param.7) | copy-start | bytes 9437188
  22.9 10.2 %copy-start.2 = (s32[1,8,12,128]{3,2,1,0:T(8,128)S(1)}, s32[1,8,12,128]{3,2,1,0:T(8,128)}, u32[]{:S(2)}) copy-start(s32[1,8,12,128]{3,2,1,0:T(8,128)} %add_bitcast_fusion) | copy-start | bytes 147460
  50.5 48.5 %all-to-all-start.4 = ((bf16[8,216,512]{2,1,0:T(8,128)(2,1)}), bf16[8,216,512]{2,1,0:T(8,128)(2,1)S(1)}, u32[]{:S(2)}, u32[]{:S(2)}) async-start(bf16[8,216,512]{2,1,0:T(8,128)(2,1)} %constant_dynamic-slice_fusion), calls=%async_computation.4 | async-start | bytes 3538944 | tf_op jit(solution)/shard_map/all_to_all | solution.py:50
  63.7 40.1 %copy-start.4 = (f32[256]{0:T(256)S(1)}, f32[256]{0:T(256)}, u32[]{:S(2)}) copy-start(f32[256]{0:T(256)} %param.10) | copy-start | bytes 3076
  99.0 16.7 %copy-start.1 = (bf16[8,216,512]{2,1,0:T(8,128)(2,1)}, bf16[8,216,512]{2,1,0:T(8,128)(2,1)S(1)}, u32[]{:S(2)}) copy-start(bf16[8,216,512]{2,1,0:T(8,128)(2,1)S(1)} %all-to-all-done.4) | copy-start | bytes 5308420
  99.0 97.1 %all-to-all-start.2 = ((bf16[8,512,512]{2,1,0:T(8,128)(2,1)}), bf16[8,512,512]{2,1,0:T(8,128)(2,1)}, u32[]{:S(2)}, u32[]{:S(2)}) async-start(bf16[8,512,512]{2,1,0:T(8,128)(2,1)} %convert_element_type.45), calls=%async_computation.2 | async-start | bytes 8388608 | tf_op jit(solution)/shard_map/all_to_all | solution.py:11
  196.2 97.0 %all-to-all-start = ((bf16[8,256,1024]{2,1,0:T(8,128)(2,1)}), bf16[8,256,1024]{2,1,0:T(8,128)(2,1)}, u32[]{:S(2)}, u32[]{:S(2)}) async-start(bf16[8,256,1024]{2,1,0:T(8,128)(2,1)} %get-tuple-element.17), calls=%async_computation | async-start | bytes 8388608 | tf_op jit(solution)/shard_map/all_to_all | solution.py:32
  200.7 171.3 %all-gather.2.cloned.1.call-start = ((), (), s32[]{:S(2)}) async-start(), calls=%async_computation.7 | async-start | bytes 8847360 | tf_op jit(solution)/shard_map/all_gather | solution.py:52
  347.0 97.6 %all-to-all-start.1 = ((bf16[8,256,1024]{2,1,0:T(8,128)(2,1)}), bf16[8,256,1024]{2,1,0:T(8,128)(2,1)}, u32[]{:S(2)}, u32[]{:S(2)}) async-start(bf16[8,256,1024]{2,1,0:T(8,128)(2,1)} %get-tuple-element.16), calls=%async_computation.1 | async-start | bytes 8388608 | tf_op jit(solution)/shard_map/all_to_all | solution.py:33
  351.5 177.1 %reduce-scatter.2.cloned.1.call-start = ((), (), s32[]{:S(2)}) async-start(), calls=%async_computation.8 | async-start | bytes 8847360 | tf_op jit(solution)/shard_map/reduce_scatter | solution.py:59
  467.2 67.0 %copy-start.3 = (f32[768,2]{0,1:T(2,128)S(1)}, f32[768,2]{0,1:T(2,128)}, u32[]{:S(2)}) copy-start(f32[768,2]{0,1:T(2,128)} %param.9) | copy-start | bytes 18436
  528.7 46.6 %all-to-all-start.5 = ((bf16[8,216,512]{2,1,0:T(8,128)(2,1)}), bf16[8,216,512]{2,1,0:T(8,128)(2,1)S(1)}, u32[]{:S(2)}, u32[]{:S(2)}) async-start(bf16[8,216,512]{2,1,0:T(8,128)(2,1)} %reduce-scatter.2.cloned.1.call-done), calls=%async_computation.6 | async-start | bytes 3538944 | tf_op jit(solution)/shard_map/all_to_all | solution.py:60
Sparse Core Ops, SparseCore 0:
  203.1 52.1 all-gather.1
  467.4 61.2 reduce-scatter.1
where the time goes:
time: 608 us; the launch traced here: 606 us
  waiting for transfers between devices  320 us (53%)
  local copies, waits for them, and re-layouts  95.9 us (16%)
  other arithmetic  59.9 us (10%)
  blocking collectives  53.8 us (9%)
  matrix products  35.3 us (6%)
  starting transfers between devices  27 us (4%)
  between operations  14.2 us (2%)
    all_to_all x1, waiting for transfers between devices, relay_down(): lax.all_to_all(down_cast, 'fs', split_axis=0, concat_axis=1, tiled=True)  80.4 us
    reduce_scatter x1, waiting for transfers between devices, body(): lax.psum_scatter(rounded.astype(jnp.bfloat16), 'tp', scatter_dimension=2,...  61.4 us
    all_to_all x1, waiting for transfers between devices, body(): lax.all_to_all(up_cast, 'fs', split_axis=0, concat_axis=1, tiled=True)  59.8 us
    all_to_all x1, blocking collectives, relay_down(): lax.all_to_all(lax.all_to_all(down_cast, 'fs', split_axis=0, concat_axis=...  53.8 us
    all_to_all x1, waiting for transfers between devices, body(): lax.all_to_all(gate_cast, 'fs', split_axis=0, concat_axis=1, tiled=True)  47.7 us
    unnamed x19, local copies, waits for them, and re-layouts  37.7 us
    all_to_all x1, waiting for transfers between devices, body(): lax.all_to_all(column_share, 'fs', split_axis=0, concat_axis=0, tiled=True)  35.3 us
    all_to_all x1, waiting for transfers between devices, body(): lax.all_to_all(summed, 'fs', split_axis=0, concat_axis=0, tiled=True)  34.4 us
  transfers between devices with their start and end apart: 7, of which 6 were waited for; matrix products, arithmetic and copies ran while one was open for 17% of the time, Pallas kernels for 0%

commit v1 on v0

v1 whole, which is shorter than its diff:
```python
import jax
import jax.numpy as jnp
from jax import lax
from jax.experimental import pallas as pl
from jax.sharding import PartitionSpec as P


CAP = 216
CHUNKS = 2


def copy_kernel(source, target):
    target[...] = source[...]


def settled(value):
    rows, columns = value.shape
    spec = pl.BlockSpec((rows // 8, columns), lambda i: (i, 0))
    return pl.pallas_call(
        copy_kernel,
        grid=(8,),
        out_shape=jax.ShapeDtypeStruct(value.shape, value.dtype),
        in_specs=[spec],
        out_specs=spec,
        cost_estimate=pl.CostEstimate(
            flops=0, bytes_accessed=2 * value.size * value.dtype.itemsize, transcendentals=0
        ),
    )(value)


def added(kept, got):
    return [
        (k.astype(jnp.float32) + g.astype(jnp.float32)).astype(jnp.bfloat16)
        for k, g in zip(kept, got)
    ]


def flip(value, bit):
    count = lax.axis_size("tp")
    return lax.ppermute(value, "tp", [(i, i ^ bit) for i in range(count)])


def gather_columns(value):
    index = lax.axis_index("tp")
    bit = lax.axis_size("tp") // 2
    pieces = [value]
    while bit:
        others = [flip(piece, bit) for piece in pieces]
        high = (index // bit) % 2 == 1
        merged = []
        for piece, other in zip(pieces, others):
            merged += [jnp.where(high, other, piece), jnp.where(high, piece, other)]
        pieces = merged
        bit //= 2
    return jnp.concatenate(pieces, axis=1)


def send_down(down_master, rounds):
    n_fs, n_tp = lax.axis_size("fs"), lax.axis_size("tp")
    ratio = n_fs // n_tp
    mine = (lax.axis_index("fs") % ratio) * n_tp + lax.axis_index("tp")
    blocks = []
    for j in rounds:
        pairs = []
        for fs in range(n_fs):
            for tp in range(n_tp):
                expert = ((fs % ratio) * n_tp + tp) ^ j
                pairs.append((fs * n_tp + tp, expert * n_tp + fs // ratio))
        block = lax.dynamic_index_in_dim(down_master, mine ^ j, 0, keepdims=False).astype(jnp.bfloat16)
        blocks.append(lax.ppermute(block, ("fs", "tp"), pairs))
    return blocks


def collect_down(blocks):
    s = lax.axis_index("fs")
    out = jnp.zeros((len(blocks),) + blocks[0].shape, blocks[0].dtype)
    for j, block in enumerate(blocks):
        out = lax.dynamic_update_slice(out, block[None], (s ^ j, 0, 0))
    return out


def body(tokens, routes, route_weight, norm_gain, gate_master, up_master, down_master):
    rows_local = tokens.shape[0]
    model_width = tokens.shape[1]
    experts = gate_master.shape[0]
    n_tp = lax.axis_size("tp")
    n_fs = lax.axis_size("fs")
    column_count = model_width // n_tp
    tp = lax.axis_index("tp")

    row_gain = norm_gain[None, :, None]
    blocks = send_down(down_master, range(n_fs))
    gate_cast = (row_gain * gate_master).astype(jnp.bfloat16)
    gate_cast, up_master = lax.optimization_barrier((gate_cast, up_master))
    gate_serve = lax.all_to_all(gate_cast, "fs", split_axis=0, concat_axis=1, tiled=True)

    values = tokens.astype(jnp.float32)
    scale = lax.rsqrt(jnp.mean(values * values, axis=-1, keepdims=True) + 1e-06)
    share = lax.dynamic_slice_in_dim(tokens, tp * column_count, column_count, 1)
    normed = (share.astype(jnp.float32) * scale).astype(jnp.bfloat16)
    chosen = routes.reshape(-1)
    one_hot = (chosen[:, None] == jnp.arange(experts, dtype=jnp.int32)[None, :]).astype(jnp.int32)
    earlier = jnp.cumsum(one_hot, axis=0) - one_hot
    position = jnp.sum(earlier * one_hot, axis=1)
    slots = (chosen * CAP + position).reshape(rows_local, 2)
    first, second = slots[:, 0], slots[:, 1]
    slot_ids = jnp.arange(experts * CAP, dtype=jnp.int32)
    picks = ((first[None, :] == slot_ids[:, None]) | (second[None, :] == slot_ids[:, None])).astype(jnp.bfloat16)
    outgoing = jnp.dot(picks, normed, preferred_element_type=jnp.float32).astype(jnp.bfloat16)
    outgoing = outgoing.reshape(experts, CAP, column_count)
    outgoing, gate_serve = lax.optimization_barrier((outgoing, gate_serve))
    arrived = lax.all_to_all(outgoing, "fs", split_axis=0, concat_axis=0, tiled=True)
    up_cast = (row_gain * up_master).astype(jnp.bfloat16)
    up_cast, arrived = lax.optimization_barrier((up_cast, arrived))
    up_serve = lax.all_to_all(up_cast, "fs", split_axis=0, concat_axis=1, tiled=True)
    incoming = gather_columns(arrived.reshape(-1, column_count))

    gate_matrix = settled(gate_serve[0])
    up_matrix = settled(up_serve[0])
    gate_pre = jnp.dot(incoming, gate_matrix, preferred_element_type=jnp.float32)
    up_pre = jnp.dot(incoming, up_serve[0], preferred_element_type=jnp.float32)
    hidden = (jax.nn.silu(gate_pre) * up_pre).astype(jnp.bfloat16)

    piece = column_count // CHUNKS
    stored = collect_down(blocks)
    part_rows = stored.shape[1]
    ratio = n_fs // n_tp
    units = ratio * part_rows
    pairs = stored.reshape(ratio, n_tp // 2, 2, part_rows, column_count)

    def joined(part):
        return part.transpose(0, 2, 1, 3).reshape(units, -1)

    down_matrix = joined(stored.reshape(ratio, n_tp, part_rows, column_count))
    core = tp % 2
    far = joined(lax.dynamic_index_in_dim(pairs, 1 - core, 2, keepdims=False))
    near = joined(lax.dynamic_index_in_dim(pairs, core, 2, keepdims=False))
    far_part = jnp.dot(hidden, far, preferred_element_type=jnp.float32).astype(jnp.bfloat16)
    other = flip(far_part, 1)
    near_part = jnp.dot(hidden, near, preferred_element_type=jnp.float32).astype(jnp.bfloat16)
    total = (near_part.astype(jnp.float32) + other.astype(jnp.float32)).astype(jnp.bfloat16)
    owners, bit = n_tp // 2, n_tp // 2
    totals = [
        [total[:, o * column_count + c * piece : o * column_count + (c + 1) * piece] for o in range(owners)]
        for c in range(CHUNKS)
    ]
    received = {}
    while owners > 1:
        high = (tp // bit) % 2 == 1
        half = owners // 2
        for c in range(CHUNKS):
            low_part, high_part = totals[c][:half], totals[c][half:]
            kept = [jnp.where(high, h, l) for l, h in zip(low_part, high_part)]
            sent = [jnp.where(high, l, h) for l, h in zip(low_part, high_part)]
            got = [flip(x, bit) for x in sent]
            received[c] = (kept, got)
        if half > 1:
            totals = [added(*received[c]) for c in range(CHUNKS)]
        owners, bit = half, bit // 2
    outputs = []
    for c in range(CHUNKS):
        kept, got = received[c]
        if c:
            got, outputs[-1], up_matrix = lax.optimization_barrier((got, outputs[-1], up_matrix))
        total = added(kept, got)[0]
        total = total.reshape(n_fs, CAP, piece)
        returned = lax.all_to_all(total, "fs", split_axis=0, concat_axis=0, tiled=True)
        returned = returned.reshape(experts * CAP, piece)
        pick_first = (first[:, None] == slot_ids[None, :]).astype(jnp.bfloat16)
        pick_second = (second[:, None] == slot_ids[None, :]).astype(jnp.bfloat16)
        outputs.append(returned)
    columns = []
    for returned in outputs:
        one = jnp.dot(pick_first, returned, preferred_element_type=jnp.float32)
        two = jnp.dot(pick_second, returned, preferred_element_type=jnp.float32)
        columns.append(one * route_weight[:, :1] + two * route_weight[:, 1:])
    combined = jnp.concatenate(columns, axis=1).astype(jnp.bfloat16)
    return (gate_matrix[None], up_matrix[None], down_matrix[None], combined)


def solution(mesh):
    placed = (
        P("fs", None),
        P("fs", None),
        P("fs", None),
        P("fs"),
        P(None, "fs", "tp"),
        P(None, "fs", "tp"),
        P(None, "fs", "tp"),
    )

    return jax.shard_map(
        body,
        mesh=mesh,
        in_specs=placed,
        out_specs=(P("fs", None, "tp"), P("fs", None, "tp"), P("fs", "tp", None), P("fs", "tp")),
        check_vma=False,
    )
```

time: 608 us -> 539 us (0.89)
  starting transfers between devices: 27 us -> 248 us
  waiting for transfers between devices: 320 us -> 165 us
  local copies, waits for them, and re-layouts: 95.9 us -> 38.6 us
  blocking collectives: 53.8 us -> 0 us
  other arithmetic: 59.9 us -> 30.4 us
  Pallas kernels: 0 us -> 13.2 us
  between operations: 14.2 us -> 1.22 us
    ppermute x0 -> x14, starting transfers between devices: none -> 222 us  [the longest x8 155 us: send_down(): blocks.append(lax.ppermute(block, ('fs', 'tp'), pairs))]
    all_to_all x3, waiting for transfers between devices: 150 us -> 36.9 us  [the longest x1 34.6 us: body(): lax.all_to_all(outgoing, 'fs', split_axis=0, concat_axis=0, tiled=True)]
    reduce_scatter x1 -> x0, waiting for transfers between devices: 61.4 us -> none  [body(): lax.psum_scatter(rounded.astype(jnp.bfloat16), 'tp', scatter_dimension=2,...]
    all_to_all x1, waiting for transfers between devices: 59.8 us -> 0.01 us  [body(): lax.all_to_all(up_cast, 'fs', split_axis=0, concat_axis=1, tiled=True)]
    all_to_all x1 -> x0, blocking collectives: 53.8 us -> none  [relay_down(): lax.all_to_all(lax.all_to_all(down_cast, 'fs', split_axis=0, concat_axis=...]
    ppermute x0 -> x14, waiting for transfers between devices: none -> 42.9 us  [the longest x6 37.9 us: flip(): return lax.ppermute(value, 'tp', [(i, i ^ bit) for i in range(count)])]
    all_to_all x1, waiting for transfers between devices: 47.7 us -> 84.9 us  [body(): lax.all_to_all(gate_cast, 'fs', split_axis=0, concat_axis=1, tiled=True)]
    unnamed x19 -> x32, local copies, waits for them, and re-layouts: 37.7 us -> 7.35 us
  transfers between devices with their start and end apart: 7 -> 19, of which waited for: 6 -> 9; matrix products, arithmetic and copies ran while one was open for 17% -> 13% of each run, Pallas kernels for 0% -> 2%
where the time goes in v1:
time: 539 us; the launch traced here: 537 us
  starting transfers between devices  248 us (46%)
  waiting for transfers between devices  165 us (31%)
  matrix products  41.2 us (8%)
  local copies, waits for them, and re-layouts  38.6 us (7%)
  other arithmetic  30.4 us (6%)
  Pallas kernels  13.2 us (2%)
    ppermute x8, starting transfers between devices, send_down(): blocks.append(lax.ppermute(block, ('fs', 'tp'), pairs))  155 us
    all_to_all x1, waiting for transfers between devices, body(): lax.all_to_all(gate_cast, 'fs', split_axis=0, concat_axis=1, tiled=True)  84.9 us
    ppermute x6, starting transfers between devices, flip(): return lax.ppermute(value, 'tp', [(i, i ^ bit) for i in range(count)])  67.1 us
    ppermute x6, waiting for transfers between devices, flip(): return lax.ppermute(value, 'tp', [(i, i ^ bit) for i in range(count)])  37.9 us
    all_to_all x1, waiting for transfers between devices, body(): lax.all_to_all(outgoing, 'fs', split_axis=0, concat_axis=0, tiled=True)  34.6 us
    pallas_call x2, Pallas kernels, settled(): pl.pallas_call(copy_kernel, grid=(8,), out_shape=jax.ShapeDtypeStruct(val...  13.2 us
    dot_general x1, matrix products, body(): up_pre = jnp.dot(incoming, up_serve[0], preferred_element_type=jnp.float32)  12.5 us
  transfers between devices with their start and end apart: 19, of which 9 were waited for; matrix products, arithmetic and copies ran while one was open for 13% of the time, Pallas kernels for 2%

profile of v1, /device:TPU:0, one launch (start us, length us, event | category | flops | bytes accessed | tf_op | source)
XLA Modules:
  0.0 537.4 jit_solution(17535481044983408926)
XLA Ops:
  0.6 6.8 %multiply_convert_fusion.1 = bf16[8,256,1024]{2,1,0:T(8,128)(2,1)} fusion(f32[8,256,1024]{2,1,0:T(8,128)} %param.11, f32[256]{0:T(256)} %param.10), kind=kLoop, calls=%fused_computation.1 | loop fusion | flops 4194304 | bytes 12583936 | tf_op jit(solution)/shard_map/convert_element_type | solution.py:93
  7.5 7.6 %all-to-all-start = ((bf16[8,256,1024]{2,1,0:T(8,128)(2,1)}), bf16[8,256,1024]{2,1,0:T(8,128)(2,1)}, u32[]{:S(2)}, u32[]{:S(2)}) async-start(bf16[8,256,1024]{2,1,0:T(8,128)(2,1)} %multiply_convert_fusion.1), calls=%async_computation | async-start | bytes 8388608 | tf_op jit(solution)/shard_map/all_to_all | solution.py:95
  15.7 2.3 reduce-window.6
  18.6 0.3 reduce_sum.21
  19.1 0.7 multiply_add_fusion
  19.8 0.7 multiply_reduce_fusion
  20.5 2.9 fusion.7
  23.5 84.9 %all-to-all-done = bf16[8,256,1024]{2,1,0:T(8,128)(2,1)} async-done(((bf16[8,256,1024]{2,1,0:T(8,128)(2,1)}), bf16[8,256,1024]{2,1,0:T(8,128)(2,1)}, u32[]{:S(2)}, u32[]{:S(2)}) %all-to-all-start) | async-done | bytes 4194336 | tf_op jit(solution)/shard_map/all_to_all | solution.py:95
  108.3 3.6 all-to-all-start.1
  112.0 6.8 %multiply_convert_fusion = bf16[8,256,1024]{2,1,0:T(8,128)(2,1)} fusion(f32[8,256,1024]{2,1,0:T(8,128)} %param.12, f32[256]{0:T(256)S(1)} %copy-done.13), kind=kLoop, calls=%fused_computation | loop fusion | flops 4194304 | bytes 12583936 | tf_op jit(solution)/shard_map/convert_element_type | solution.py:113
  118.7 34.6 %all-to-all-done.1 = bf16[8,216,512]{2,1,0:T(8,128)(2,1)S(1)} async-done(((bf16[8,216,512]{2,1,0:T(8,128)(2,1)}), bf16[8,216,512]{2,1,0:T(8,128)(2,1)S(1)}, u32[]{:S(2)}, u32[]{:S(2)}) %all-to-all-start.1) | async-done | bytes 1769504 | tf_op jit(solution)/shard_map/all_to_all | solution.py:112
  153.4 1.5 collective-permute-start
  154.8 4.5 all-to-all-start.2
  159.4 5.5 %fusion.35 = (bf16[512,512]{1,0:T(8,128)(2,1)}, bf16[512,512]{1,0:T(8,128)(2,1)}, bf16[512,512]{1,0:T(8,128)(2,1)}, bf16[512,512]{1,0:T(8,128)(2,1)}, bf16[512,5...) fusion(f32[8,512,512]{2,1,0:T(8,128)} %param.13, ...), kind=kLoop, calls=%fused_computation.64 | loop fusion | bytes 8388640 | tf_op jit(solution)/shard_map/convert_element_type | solution.py:69
  164.9 5.4 collective-permute-start.3
  170.3 0.8 collective-permute-start.4
  171.1 1.2 collective-permute-start.5
  172.3 4.9 collective-permute-start.6
  177.3 132.4 %collective-permute-start.7 = (bf16[512,512]{1,0:T(8,128)(2,1)}, bf16[512,512]{1,0:T(8,128)(2,1)S(1)}, u32[]{:S(2)}, u32[]{:S(2)}) collective-permute-start(bf16[512,512]{1,0:T(8,128)(2,1)} %get-tuple-element.44), channel_id=1, source_target_pairs={{0,16},{1,20},{2,24},{3,28},{4,0},{5,4},{6,8},{7,12},{8,17},{9,21}... | collective-permute-start | bytes 1572872 | tf_op jit(solution)/shard_map/ppermute | solution.py:70
  309.7 0.4 broadcast_in_dim.41
  310.0 1.1 bitcast_dynamic-update-slice_fusion.7
  311.1 7.2 %collective-permute-start.8 = (bf16[512,512]{1,0:T(8,128)(2,1)S(1)}, bf16[512,512]{1,0:T(8,128)(2,1)S(1)}, u32[]{:S(2)}, u32[]{:S(2)}) collective-permute-start(bf16[512,512]{1,0:T(8,128)(2,1)S(1)} %copy-done.10), channel_id=1, source_target_pairs={{0,20},{1,16},{2,28},{3,24},{4,4},{5,0},{6,12},{7,8},{8,21},{9,17}... | collective-permute-start | bytes 1572872 | tf_op jit(solution)/shard_map/ppermute | solution.py:70
  318.4 2.1 broadcast_select_fusion.1
  320.5 1.1 bitcast_dynamic-update-slice_fusion.6
  321.6 2.8 collective-permute-start.9
  324.4 1.1 bitcast_dynamic-update-slice_fusion.5
  325.7 1.1 bitcast_dynamic-update-slice_fusion.4
  326.8 18.8 %collective-permute-start.1 = (bf16[1728,512]{1,0:T(8,128)(2,1)}, bf16[1728,512]{1,0:T(8,128)(2,1)}, u32[]{:S(2)}, u32[]{:S(2)}) collective-permute-start(bf16[1728,512]{1,0:T(8,128)(2,1)} %get-tuple-element.56), channel_id=1, source_target_pairs={{0,1},{1,0},{2,3},{3,2},{4,5},{5,4},{6,7},{7,6},{8,9},{9,8},{10,11... | collective-permute-start | bytes 5308424 | tf_op jit(solution)/shard_map/ppermute | solution.py:40
  345.7 3.4 collective-permute-done.9
  349.2 1.6 collective-permute-done.10
  351.1 1.7 copy-done
  352.8 2.2 copy.31
  355.0 1.9 copy.36
  356.9 6.6 %shard_map.102 = bf16[2048,1024]{1,0:T(8,128)(2,1)} custom-call(bf16[2048,1024]{1,0:T(8,128)(2,1)} %bitcast.3.source), custom_call_target="tpu_custom_call" | custom-call | bytes 8388608 | tf_op jit(solution)/shard_map/pallas_call | solution.py:19
  363.5 2.2 broadcast_select_fusion.3
  365.8 3.5 broadcast_select_fusion.5
  369.3 1.2 copy-done.6
  370.6 0.5 copy-done.7
  371.1 9.4 %fusion.25 = f32[1728,1024]{1,0:T(8,128)} fusion(bf16[2048,1024]{1,0:T(8,128)(2,1)S(1)} %copy-done.1, bf16[1728,512]{1,0:T(8,128)(2,1)S(1)} %get-tuple-element.59, bf16[1728,512]{1,0:T(8,128)(2,1)S(1)} %get-tuple-element.58, bf16[1728,512]{1,0:T(8,128)(2,1)S(1)} %get-tuple-element.55, bf16[1728,512]{1,0:T(8,128)(2,1)S(1)} %get-tuple-element.54), kind=kOutput, calls=%fused_computation.43 | convolution fusion | flops 7276068864 | bytes 18350080 | tf_op jit(solution)/shard_map/dot_general | solution.py:120
  380.5 12.5 %multiply_convert_fusion.2 = bf16[1728,1024]{1,0:T(8,128)(2,1)S(1)} fusion(f32[1728,1024]{1,0:T(8,128)} %fusion.25, bf16[2048,1024]{1,0:T(8,128)(2,1)} %bitcast.6.source, bf16[1728,512]{1,0:T(8,128)(2,1)} %copy-done.5, bf16[1728,512]{1,0:T(8,128)(2,1)} %copy-done.4, bf16[1728,512]{1,0:T(8,128)(2,1)} %copy-done.7, bf16[1728,512]{1,0:T(8,128)(2,1)} %copy-done.6), kind=kOutput, calls=%fused_computation.4 | convolution fusion | flops 7286685696 | bytes 21889024 | tf_op jit(solution)/shard_map/dot_general | solution.py:121
  393.1 4.0 convolution_convert_fusion
  397.1 45.1 %collective-permute-start.11 = (bf16[1728,1024]{1,0:T(8,128)(2,1)S(1)}, bf16[1728,1024]{1,0:T(8,128)(2,1)S(1)}, u32[]{:S(2)}, u32[]{:S(2)}) collective-permute-start(bf16[1728,1024]{1,0:T(8,128)(2,1)S(1)} %convolution_convert_fusion), channel_id=1, source_target_pairs={{0,1},{1,0},{2,3},{3,2},{4,5},{5,4},{6,7},{7,6},{8,9},{9,8},{10,11... | collective-permute-start | bytes 10616840 | tf_op jit(solution)/shard_map/ppermute | solution.py:40
  442.2 2.2 copy.30
  444.3 0.6 copy.35
  444.9 3.1 collective-permute-done.11
  448.0 4.3 add_convert_fusion
  452.3 1.1 broadcast_select_fusion.6
  453.4 21.9 %collective-permute-done.13 = bf16[1728,256]{1,0:T(8,128)(2,1)S(1)} collective-permute-done((bf16[1728,256]{1,0:T(8,128)(2,1)S(1)}, bf16[1728,256]{1,0:T(8,128)(2,1)S(1)}, u32[]{:S(2)}, u32[]{:S(2)}) %collective-permute-start.13) | collective-permute-done | bytes 884768 | tf_op jit(solution)/shard_map/ppermute | solution.py:40
  475.3 1.3 add_convert_fusion.2
  476.7 5.9 %all-to-all-start.3 = ((bf16[8,216,256]{2,1,0:T(8,128)(2,1)}), bf16[8,216,256]{2,1,0:T(8,128)(2,1)}, u32[]{:S(2)}, u32[]{:S(2)}) async-start(bf16[8,216,256]{2,1,0:T(8,128)(2,1)} %bitcast.98), calls=%async_computation.3 | async-start | bytes 1769472 | tf_op jit(solution)/shard_map/all_to_all | solution.py:167
  482.5 1.7 collective-permute-start.12
  484.3 6.6 %shard_map.103 = bf16[2048,1024]{1,0:T(8,128)(2,1)} custom-call(bf16[2048,1024]{1,0:T(8,128)(2,1)} %bitcast.6.source), custom_call_target="tpu_custom_call" | custom-call | bytes 8388608 | tf_op jit(solution)/shard_map/pallas_call | solution.py:19
  490.9 12.8 %collective-permute-done.12 = bf16[1728,256]{1,0:T(8,128)(2,1)} collective-permute-done((bf16[1728,256]{1,0:T(8,128)(2,1)}, bf16[1728,256]{1,0:T(8,128)(2,1)}, u32[]{:S(2)}, u32[]{:S(2)}) %collective-permute-start.12) | collective-permute-done | bytes 884768 | tf_op jit(solution)/shard_map/ppermute | solution.py:40
  503.7 1.2 all-to-all-done.3
  504.8 2.5 add_convert_fusion.1
  507.3 4.6 all-to-all-start.4
  511.9 7.4 %copy.32 = bf16[2,512,4,512]{3,2,1,0:T(4,128)(2,1)} copy(bf16[2,512,4,512]{3,1,2,0:T(8,128)(2,1)} %bitcast.91) | data formatting | bytes 8388608 | tf_op jit(solution)/shard_map/transpose | solution.py:132
  519.3 7.7 %broadcast_in_dim_reshape.4 = bf16[1,1024,2048]{2,1,0:T(8,128)(2,1)} reshape(bf16[2,512,4,512]{3,2,1,0:T(4,128)(2,1)} %copy.32) | data formatting | bytes 8388608 | tf_op jit(solution)/shard_map/broadcast_in_dim;reshape | solution.py:178
  527.0 2.6 fusion.18
  529.6 2.6 fusion.22
  532.2 1.1 all-to-all-done.4
  533.3 1.4 fusion.17
  534.7 1.4 fusion.23
  536.2 1.2 copy.33
  (56 shorter events, 2.2 us)
Async XLA Ops:
  7.5 7.6 %copy-start.11 = (s32[768,2]{0,1:T(2,128)S(1)}, s32[768,2]{0,1:T(2,128)}, u32[]{:S(2)}) copy-start(s32[768,2]{0,1:T(2,128)} %param.8) | copy-start | bytes 18436
  7.5 12.3 %copy-start.2 = (bf16[768,2048]{1,0:T(8,128)(2,1)S(1)}, bf16[768,2048]{1,0:T(8,128)(2,1)}, u32[]{:S(2)}) copy-start(bf16[768,2048]{1,0:T(8,128)(2,1)} %param.7) | copy-start | bytes 9437188
  7.5 100.9 %all-to-all-start = ((bf16[8,256,1024]{2,1,0:T(8,128)(2,1)}), bf16[8,256,1024]{2,1,0:T(8,128)(2,1)}, u32[]{:S(2)}, u32[]{:S(2)}) async-start(bf16[8,256,1024]{2,1,0:T(8,128)(2,1)} %multiply_convert_fusion.1), calls=%async_computation | async-start | bytes 8388608 | tf_op jit(solution)/shard_map/all_to_all | solution.py:95
  20.5 91.5 %copy-start.13 = (f32[256]{0:T(256)S(1)}, f32[256]{0:T(256)}, u32[]{:S(2)}) copy-start(f32[256]{0:T(256)} %param.10) | copy-start | bytes 3076
  108.3 45.0 %all-to-all-start.1 = ((bf16[8,216,512]{2,1,0:T(8,128)(2,1)}), bf16[8,216,512]{2,1,0:T(8,128)(2,1)S(1)}, u32[]{:S(2)}, u32[]{:S(2)}) async-start(bf16[8,216,512]{2,1,0:T(8,128)(2,1)} %bitcast.101), calls=%async_computation.1 | async-start | bytes 3538944 | tf_op jit(solution)/shard_map/all_to_all | solution.py:112
  153.4 157.8 %collective-permute-start = (bf16[1728,512]{1,0:T(8,128)(2,1)S(1)}, bf16[1728,512]{1,0:T(8,128)(2,1)S(1)}, u32[]{:S(2)}, u32[]{:S(2)}) collective-permute-start(bf16[1728,512]{1,0:T(8,128)(2,1)S(1)} %bitcast.94), channel_id=1, source_target_pairs={{0,2},{1,3},{2,0},{3,1},{4,6},{5,7},{6,4},{7,5},{8,10},{9,11},{10,... | collective-permute-start | bytes 5308424 | tf_op jit(solution)/shard_map/ppermute | solution.py:40
  154.8 225.7 %all-to-all-start.2 = ((bf16[8,256,1024]{2,1,0:T(8,128)(2,1)}), bf16[8,256,1024]{2,1,0:T(8,128)(2,1)}, u32[]{:S(2)}, u32[]{:S(2)}) async-start(bf16[8,256,1024]{2,1,0:T(8,128)(2,1)} %multiply_convert_fusion), calls=%async_computation.2 | async-start | bytes 8388608 | tf_op jit(solution)/shard_map/all_to_all | solution.py:115
  164.9 12.3 %collective-permute-start.3 = (bf16[512,512]{1,0:T(8,128)(2,1)}, bf16[512,512]{1,0:T(8,128)(2,1)}, u32[]{:S(2)}, u32[]{:S(2)}) collective-permute-start(bf16[512,512]{1,0:T(8,128)(2,1)} %get-tuple-element.48), channel_id=1, source_target_pairs={{0,0},{1,4},{2,8},{3,12},{4,16},{5,20},{6,24},{7,28},{8,1},{9,5},{... | collective-permute-start | bytes 1572872 | tf_op jit(solution)/shard_map/ppermute | solution.py:70
  170.3 150.2 %collective-permute-start.4 = (bf16[512,512]{1,0:T(8,128)(2,1)}, bf16[512,512]{1,0:T(8,128)(2,1)}, u32[]{:S(2)}, u32[]{:S(2)}) collective-permute-start(bf16[512,512]{1,0:T(8,128)(2,1)} %get-tuple-element.47), channel_id=1, source_target_pairs={{0,4},{1,0},{2,12},{3,8},{4,20},{5,16},{6,28},{7,24},{8,5},{9,1},{... | collective-permute-start | bytes 1572872 | tf_op jit(solution)/shard_map/ppermute | solution.py:70
  171.1 150.5 %collective-permute-start.5 = (bf16[512,512]{1,0:T(8,128)(2,1)}, bf16[512,512]{1,0:T(8,128)(2,1)}, u32[]{:S(2)}, u32[]{:S(2)}) collective-permute-start(bf16[512,512]{1,0:T(8,128)(2,1)} %get-tuple-element.46), channel_id=1, source_target_pairs={{0,8},{1,12},{2,0},{3,4},{4,24},{5,28},{6,16},{7,20},{8,9},{9,13},... | collective-permute-start | bytes 1572872 | tf_op jit(solution)/shard_map/ppermute | solution.py:70
  172.3 153.2 %collective-permute-start.6 = (bf16[512,512]{1,0:T(8,128)(2,1)}, bf16[512,512]{1,0:T(8,128)(2,1)}, u32[]{:S(2)}, u32[]{:S(2)}) collective-permute-start(bf16[512,512]{1,0:T(8,128)(2,1)} %get-tuple-element.45), channel_id=1, source_target_pairs={{0,12},{1,8},{2,4},{3,0},{4,28},{5,24},{6,20},{7,16},{8,13},{9,9},... | collective-permute-start | bytes 1572872 | tf_op jit(solution)/shard_map/ppermute | solution.py:70
  177.2 133.9 %copy-start.10 = (bf16[512,512]{1,0:T(8,128)(2,1)S(1)}, bf16[512,512]{1,0:T(8,128)(2,1)}, u32[]{:S(2)}) copy-start(bf16[512,512]{1,0:T(8,128)(2,1)} %get-tuple-element.43) | copy-start | bytes 1572868
  177.3 149.6 %collective-permute-start.7 = (bf16[512,512]{1,0:T(8,128)(2,1)}, bf16[512,512]{1,0:T(8,128)(2,1)S(1)}, u32[]{:S(2)}, u32[]{:S(2)}) collective-permute-start(bf16[512,512]{1,0:T(8,128)(2,1)} %get-tuple-element.44), channel_id=1, source_target_pairs={{0,16},{1,20},{2,24},{3,28},{4,0},{5,4},{6,8},{7,12},{8,17},{9,21}... | collective-permute-start | bytes 1572872 | tf_op jit(solution)/shard_map/ppermute | solution.py:70
  311.1 10.5 %copy-start.9 = (bf16[512,512]{1,0:T(8,128)(2,1)S(1)}, bf16[512,512]{1,0:T(8,128)(2,1)}, u32[]{:S(2)}) copy-start(bf16[512,512]{1,0:T(8,128)(2,1)} %get-tuple-element.49) | copy-start | bytes 1572868
  311.1 14.4 %copy-start.8 = (bf16[512,512]{1,0:T(8,128)(2,1)S(1)}, bf16[512,512]{1,0:T(8,128)(2,1)}, u32[]{:S(2)}) copy-start(bf16[512,512]{1,0:T(8,128)(2,1)} %get-tuple-element.42) | copy-start | bytes 1572868
  311.1 34.5 %collective-permute-start.8 = (bf16[512,512]{1,0:T(8,128)(2,1)S(1)}, bf16[512,512]{1,0:T(8,128)(2,1)S(1)}, u32[]{:S(2)}, u32[]{:S(2)}) collective-permute-start(bf16[512,512]{1,0:T(8,128)(2,1)S(1)} %copy-done.10), channel_id=1, source_target_pairs={{0,20},{1,16},{2,28},{3,24},{4,4},{5,0},{6,12},{7,8},{8,21},{9,17}... | collective-permute-start | bytes 1572872 | tf_op jit(solution)/shard_map/ppermute | solution.py:70
  320.5 43.0 %collective-permute-start.2 = (bf16[1728,512]{1,0:T(8,128)(2,1)}, bf16[1728,512]{1,0:T(8,128)(2,1)}, u32[]{:S(2)}, u32[]{:S(2)}) collective-permute-start(bf16[1728,512]{1,0:T(8,128)(2,1)} %get-tuple-element.57), channel_id=1, source_target_pairs={{0,1},{1,0},{2,3},{3,2},{4,5},{5,4},{6,7},{7,6},{8,9},{9,8},{10,11... | collective-permute-start | bytes 5308424 | tf_op jit(solution)/shard_map/ppermute | solution.py:40
  321.6 27.5 %collective-permute-start.9 = (bf16[512,512]{1,0:T(8,128)(2,1)S(1)}, bf16[512,512]{1,0:T(8,128)(2,1)S(1)}, u32[]{:S(2)}, u32[]{:S(2)}) collective-permute-start(bf16[512,512]{1,0:T(8,128)(2,1)S(1)} %copy-done.9), channel_id=1, source_target_pairs={{0,24},{1,28},{2,16},{3,20},{4,8},{5,12},{6,0},{7,4},{8,25},{9,29}... | collective-permute-start | bytes 1572872 | tf_op jit(solution)/shard_map/ppermute | solution.py:70
  325.5 25.3 %collective-permute-start.10 = (bf16[512,512]{1,0:T(8,128)(2,1)S(1)}, bf16[512,512]{1,0:T(8,128)(2,1)S(1)}, u32[]{:S(2)}, u32[]{:S(2)}) collective-permute-start(bf16[512,512]{1,0:T(8,128)(2,1)S(1)} %copy-done.8), channel_id=1, source_target_pairs={{0,28},{1,24},{2,20},{3,16},{4,12},{5,8},{6,4},{7,0},{8,29},{9,25}... | collective-permute-start | bytes 1572872 | tf_op jit(solution)/shard_map/ppermute | solution.py:70
  326.8 38.9 %collective-permute-start.1 = (bf16[1728,512]{1,0:T(8,128)(2,1)}, bf16[1728,512]{1,0:T(8,128)(2,1)}, u32[]{:S(2)}, u32[]{:S(2)}) collective-permute-start(bf16[1728,512]{1,0:T(8,128)(2,1)} %get-tuple-element.56), channel_id=1, source_target_pairs={{0,1},{1,0},{2,3},{3,2},{4,5},{5,4},{6,7},{7,6},{8,9},{9,8},{10,11... | collective-permute-start | bytes 5308424 | tf_op jit(solution)/shard_map/ppermute | solution.py:40
  350.8 2.0 copy-start
  365.7 3.6 copy-start.4
  365.7 3.6 copy-start.5
  365.7 5.4 copy-start.1
  369.3 1.3 copy-start.6
  369.3 1.8 copy-start.7
  380.5 12.5 %copy-start.3 = (bf16[128,8,2,512]{3,1,2,0:T(8,128)(2,1)S(1)}, bf16[128,8,2,512]{3,1,2,0:T(8,128)(2,1)}, u32[]{:S(2)}) copy-start(bf16[128,8,2,512]{3,1,2,0:T(8,128)(2,1)} %copy.36) | copy-start | bytes 6291460
  397.1 50.9 %collective-permute-start.11 = (bf16[1728,1024]{1,0:T(8,128)(2,1)S(1)}, bf16[1728,1024]{1,0:T(8,128)(2,1)S(1)}, u32[]{:S(2)}, u32[]{:S(2)}) collective-permute-start(bf16[1728,1024]{1,0:T(8,128)(2,1)S(1)} %convolution_convert_fusion), channel_id=1, source_target_pairs={{0,1},{1,0},{2,3},{3,2},{4,5},{5,4},{6,7},{7,6},{8,9},{9,8},{10,11... | collective-permute-start | bytes 10616840 | tf_op jit(solution)/shard_map/ppermute | solution.py:40
  453.4 21.9 %collective-permute-start.13 = (bf16[1728,256]{1,0:T(8,128)(2,1)S(1)}, bf16[1728,256]{1,0:T(8,128)(2,1)S(1)}, u32[]{:S(2)}, u32[]{:S(2)}) collective-permute-start(bf16[1728,256]{1,0:T(8,128)(2,1)S(1)} %get-tuple-element.52), channel_id=1, source_target_pairs={{0,2},{1,3},{2,0},{3,1},{4,6},{5,7},{6,4},{7,5},{8,10},{9,11},{10,... | collective-permute-start | bytes 2654216 | tf_op jit(solution)/shard_map/ppermute | solution.py:40
  476.7 28.2 %all-to-all-start.3 = ((bf16[8,216,256]{2,1,0:T(8,128)(2,1)}), bf16[8,216,256]{2,1,0:T(8,128)(2,1)}, u32[]{:S(2)}, u32[]{:S(2)}) async-start(bf16[8,216,256]{2,1,0:T(8,128)(2,1)} %bitcast.98), calls=%async_computation.3 | async-start | bytes 1769472 | tf_op jit(solution)/shard_map/all_to_all | solution.py:167
  482.5 21.1 %collective-permute-start.12 = (bf16[1728,256]{1,0:T(8,128)(2,1)}, bf16[1728,256]{1,0:T(8,128)(2,1)}, u32[]{:S(2)}, u32[]{:S(2)}) collective-permute-start(bf16[1728,256]{1,0:T(8,128)(2,1)} %get-tuple-element.53), channel_id=1, source_target_pairs={{0,2},{1,3},{2,0},{3,1},{4,6},{5,7},{6,4},{7,5},{8,10},{9,11},{10,... | collective-permute-start | bytes 2654216 | tf_op jit(solution)/shard_map/ppermute | solution.py:40
  490.8 21.0 %copy-start.12 = (f32[768,2]{0,1:T(2,128)S(1)}, f32[768,2]{0,1:T(2,128)}, u32[]{:S(2)}) copy-start(f32[768,2]{0,1:T(2,128)} %param.9) | copy-start | bytes 18436
  507.3 26.0 %all-to-all-start.4 = ((bf16[8,216,256]{2,1,0:T(8,128)(2,1)}), bf16[8,216,256]{2,1,0:T(8,128)(2,1)S(1)}, u32[]{:S(2)}, u32[]{:S(2)}) async-start(bf16[8,216,256]{2,1,0:T(8,128)(2,1)} %bitcast.97), calls=%async_computation.4 | async-start | bytes 1769472 | tf_op jit(solution)/shard_map/all_to_all | solution.py:167
